TPU v7x, 32 devices: a whole 2x2x4 slice. The times are simulated.
32 devices in a mesh: sp: 8 (over z, x), tp: 4 (over y, core).
Axes of the slice: x: 2, y: 2, z: 4, core: 2. Of those that a mesh axis runs over, the one named last changes fastest.
Arguments:
- tokens: bfloat16 [4096, 2048], P(('sp', 'tp')), may hold values from -6 to 6
- norm_gain: float32 [2048], replicated, may hold values from 0.1 to 1.9
- w_query: bfloat16 [2048, 1024], P(None, 'tp'), may hold values from -16 to 16
- w_key: bfloat16 [2048, 1024], P(None, 'tp'), may hold values from -16 to 16
- w_value: bfloat16 [2048, 1024], P(None, 'tp'), may hold values from -0.125 to 0.125
- conv_in: bfloat16 [2048, 2048], P(None, 'tp'), may hold values from -0.125 to 0.125
- conv_gate: bfloat16 [2048, 2048], P(None, 'tp'), may hold values from -0.125 to 0.125
- conv_taps: float32 [31, 2048], P(None, 'tp'), may hold values from -3.7 to 3.7
- conv_gain: float32 [2048], P('tp'), may hold values from 0.1 to 1.9
- cum_gate: float32 [16, 4096], P('tp'), may hold values from -514 to 0, as said below
- out_attn: bfloat16 [1024, 2048], P('tp'), may hold values from -0.75 to 0.75
- out_conv: bfloat16 [2048, 2048], P('tp'), may hold values from -0.125 to 0.125
Outputs:
- mixed: bfloat16 [4096, 2048], P(('sp', 'tp'))
- log_total: float32 [16, 4096], P('tp', 'sp')
Inputs may be any that keep to these rules, and one draw needn't show every extreme that they name: `cum_gate`: for each head the values never rise from one position to the next and are at most 0.
All inputs are finite; a program needn't handle non-finite values.
Results may differ from a plain program's by a relative error of at most 0.014.
Values may be sent and summed in bfloat16 or wider, within the bound.
A program may use at most 128 MiB of HBM per device.

v0:
```python
import jax
import jax.numpy as jnp
from jax import lax
from jax.sharding import PartitionSpec as P

HEAD = 64


def shifted(array, axis, by):
    length = lax.axis_size(axis)
    pairs = [(i, i + by) for i in range(length) if 0 <= i + by < length]
    return lax.ppermute(array, axis, pairs)


def per_device(
    tokens,
    norm_gain,
    w_query,
    w_key,
    w_value,
    conv_in,
    conv_gate,
    conv_taps,
    conv_gain,
    cum_gate,
    out_attn,
    out_conv,
):
    heads_here = w_query.shape[1] // HEAD
    width_att = w_query.shape[1]
    channels = conv_in.shape[1]
    kernel_len = conv_taps.shape[0]
    wide = lax.all_gather(tokens, "tp", axis=0, tiled=True).astype(jnp.float32)
    factor = lax.rsqrt(jnp.mean(wide * wide, axis=1, keepdims=True) + 1e-06)
    normed = (wide * factor * norm_gain[None, :]).astype(jnp.bfloat16)
    query = (jnp.dot(normed, w_query, preferred_element_type=jnp.float32) * HEAD ** (-0.5)).astype(
        jnp.bfloat16
    )
    keyed = jnp.dot(normed, w_key, preferred_element_type=jnp.float32).astype(jnp.bfloat16)
    valued = jnp.dot(normed, w_value, preferred_element_type=jnp.float32).astype(jnp.bfloat16)
    opened = jnp.dot(normed, conv_in, preferred_element_type=jnp.float32)
    gating = jnp.dot(normed, conv_gate, preferred_element_type=jnp.float32)
    gated_rows = (opened * jax.nn.sigmoid(gating)).astype(jnp.bfloat16)
    joined = jnp.concatenate([query, keyed, valued, gated_rows], axis=1)
    local_rows = joined.shape[0]
    own_index = lax.axis_index("sp")
    offset = own_index * local_rows
    query_rows = joined[:, :width_att]
    key_rows = joined[:, width_att : 2 * width_att]
    value_rows = joined[:, 2 * width_att : 3 * width_att]
    gated = joined[:, 3 * width_att :]
    group_list = (query_rows, offset)
    group_data = []
    group_rows, group_start = group_list
    count_rows = group_rows.shape[0]
    group_data.append(
        (
            group_rows.reshape(count_rows, heads_here, HEAD),
            lax.dynamic_slice_in_dim(cum_gate, group_start, count_rows, 1),
            group_start + jnp.arange(count_rows, dtype=jnp.int32),
            group_start + count_rows - 1,
        )
    )

    def absorb(carry_in, group, key_block, value_block, first_place):
        query_heads, cum_query, query_place, last_query = group
        row_best, row_total, row_accum = carry_in
        length_in = key_block.shape[0]
        key_heads = key_block.reshape(length_in, heads_here, HEAD)
        value_heads = value_block.reshape(length_in, heads_here, HEAD)
        cum_keys = lax.dynamic_slice_in_dim(cum_gate, first_place, length_in, 1)
        scores = jnp.einsum(
            "qhd,khd->hqk", query_heads, key_heads, preferred_element_type=jnp.float32
        )
        scores = scores + cum_query[:, :, None] - cum_keys[:, None, :]
        key_place = first_place + jnp.arange(length_in, dtype=jnp.int32)
        visible = jnp.logical_and(
            key_place[None, :] <= query_place[:, None], key_place[None, :] >= 0
        )[None]
        scores = jnp.where(visible, scores, -1e30)
        new_best = jnp.maximum(row_best, jnp.max(scores, axis=2))
        shrink = jnp.exp(row_best - new_best)
        weights = jnp.where(visible, jnp.exp(scores - new_best[:, :, None]), 0.0)
        row_total = shrink * row_total + jnp.sum(weights, axis=2)
        row_accum = shrink[:, :, None] * row_accum + jnp.einsum(
            "hqk,khd->hqd",
            weights.astype(jnp.bfloat16),
            value_heads,
            preferred_element_type=jnp.float32,
        )
        return (new_best, row_total, row_accum)

    initial = tuple(
        (
            (
                jnp.full((heads_here, group[0].shape[0]), -1e30, jnp.float32),
                jnp.zeros((heads_here, group[0].shape[0]), jnp.float32),
                jnp.zeros((heads_here, group[0].shape[0], HEAD), jnp.float32),
            )
            for group in group_data
        )
    )
    key_group = lax.all_gather(key_rows, "sp", axis=0, tiled=True)
    value_group = lax.all_gather(value_rows, "sp", axis=0, tiled=True)
    length_in = key_group.shape[0]
    turns = length_in // local_rows

    def advance(turn_index, carry_now):
        begin_row = turn_index * local_rows
        key_block = lax.dynamic_slice_in_dim(key_group, begin_row, local_rows, 0)
        value_block = lax.dynamic_slice_in_dim(value_group, begin_row, local_rows, 0)
        updated = []
        for group, inner_carry in zip(group_data, carry_now):
            wanted = jnp.logical_and(begin_row <= group[3], begin_row + local_rows > 0)

            def take_block(inner, group=group):
                return absorb(inner, group, key_block, value_block, begin_row)

            def skip_block(inner):
                return inner

            updated.append(lax.cond(wanted, take_block, skip_block, inner_carry))
        return tuple(updated)

    carry = lax.fori_loop(0, turns, advance, initial)
    attended_parts = []
    total_parts = []
    for row_best, row_total, row_accum in carry:
        count_rows = row_total.shape[1]
        attended_parts.append(
            (row_accum / row_total[:, :, None])
            .astype(jnp.bfloat16)
            .transpose(1, 0, 2)
            .reshape(count_rows, width_att)
        )
        total_parts.append(row_best + jnp.log(row_total))
    attended = attended_parts[0]
    log_total = total_parts[0]
    rim_rows = shifted(gated[local_rows - (kernel_len - 1) :], "sp", 1)
    padded = jnp.concatenate([rim_rows, gated], axis=0).astype(jnp.float32)
    convolved = jnp.zeros((local_rows, channels), jnp.float32)
    for tap_index in range(kernel_len):
        convolved = (
            convolved + conv_taps[tap_index][None, :] * padded[tap_index : tap_index + local_rows]
        )
    all_channels = channels * lax.axis_size("tp")
    channel_square = lax.psum(jnp.sum(convolved * convolved, axis=1), "tp") / all_channels
    conv_out = jax.nn.silu(
        convolved * lax.rsqrt(channel_square + 1e-06)[:, None] * conv_gain[None, :]
    ).astype(jnp.bfloat16)
    group_part = jnp.dot(attended, out_attn, preferred_element_type=jnp.float32)
    group_part = group_part + jnp.dot(conv_out, out_conv, preferred_element_type=jnp.float32)
    mixed = lax.psum_scatter(
        lax.optimization_barrier(group_part.astype(jnp.bfloat16))
        .astype(jnp.float32)
        .astype(jnp.bfloat16),
        "tp",
        scatter_dimension=0,
        tiled=True,
    )
    return (mixed, log_total)


def solution(mesh):
    in_specs = (
        P(("sp", "tp"), None),
        P(),
        P(None, "tp"),
        P(None, "tp"),
        P(None, "tp"),
        P(None, "tp"),
        P(None, "tp"),
        P(None, "tp"),
        P("tp"),
        P("tp", None),
        P("tp", None),
        P("tp", None),
    )
    out_specs = (P(("sp", "tp"), None), P("tp", "sp"))
    return jax.shard_map(
        per_device, mesh=mesh, in_specs=in_specs, out_specs=out_specs, check_vma=False
    )
```

profile of v0, /device:TPU:0, one launch (start us, length us, event | category | flops | bytes accessed | tf_op | source)
XLA Modules:
  0.0 236.0 jit_solution(1296425185891095124)
XLA Ops:
  7.2 0.0 copy-start
  7.2 0.0 all-gather.4.cloned.1.call-start
  7.2 0.7 all-gather.4.cloned.1.call-update
  7.9 0.0 copy-start.5
  7.9 0.0 copy-start.7
  7.9 0.0 all-gather.6.cloned.1.call-start
  8.0 26.9 %all-gather.4.cloned.1.call-done = bf16[512,2048]{1,0:T(8,128)(2,1)} async-done(((bf16[128,2048]{1,0:T(8,128)(2,1)}), bf16[512,2048]{1,0:T(8,128)(2,1)}) %all-gather.4.cloned.1.call-update) | async-done | bytes 2097168 | tf_op jit(solution)/shard_map/all_gather | solution.py:33
  34.9 2.1 fusion.13
  37.0 3.3 %convolution_convert_fusion.1 = bf16[512,256]{1,0:T(8,128)(2,1)} fusion(bf16[2048,256]{1,0:T(8,128)(2,1)} %param.19, bf16[512,2048]{1,0:T(8,128)(2,1)} %all-gather.4.cloned.1.call-done, f32[2048]{0:T(1024)} %param.17, f32[512]{0:T(512)S(1)} %add_rsqrt_fusion.1), kind=kOutput, calls=%fused_computation.35 | convolution fusion | flops 541196288 | bytes 3418112 | tf_op jit(solution)/shard_map/dot_general | solution.py:39
  40.3 0.0 all-gather.6.cloned.1.call-update
  40.3 0.0 all-gather.8.cloned.1.call-start
  40.4 0.0 copy-done.5
  40.4 0.0 copy-done.7
  40.4 3.0 %convolution_convert_fusion = bf16[512,256]{1,0:T(8,128)(2,1)} fusion(bf16[2048,256]{1,0:T(8,128)(2,1)S(1)} %copy-done.5, bf16[512,2048]{1,0:T(8,128)(2,1)} %all-gather.4.cloned.1.call-done, f32[2048]{0:T(1024)S(1)} %copy-done.7, f32[512]{0:T(512)S(1)} %add_rsqrt_fusion.1), kind=kOutput, calls=%fused_computation.34 | convolution fusion | flops 541196288 | bytes 3418112 | tf_op jit(solution)/shard_map/dot_general | solution.py:40
  43.4 0.0 all-gather.8.cloned.1.call-update
  43.5 0.0 reduce-scatter.2.cloned.1.call-start
  43.5 0.7 constant_dynamic-slice_fusion.3
  44.2 0.0 copy-done.3
  44.3 0.0 copy-start.1
  44.3 0.0 copy-start.4
  44.3 3.8 %fusion.18 = f32[512,512]{1,0:T(8,128)S(1)} fusion(bf16[2048,512]{1,0:T(8,128)(2,1)} %param.22, bf16[512,2048]{1,0:T(8,128)(2,1)} %all-gather.4.cloned.1.call-done, f32[2048]{0:T(1024)S(1)} %copy-done.7, f32[512]{0:T(512)S(1)} %add_rsqrt_fusion.1), kind=kOutput, calls=%fused_computation.30 | convolution fusion | flops 1078722560 | bytes 5253120 | tf_op jit(solution)/shard_map/dot_general | solution.py:42
  48.1 0.0 copy-start.6
  48.2 1.3 fusion.19
  49.5 3.4 %collective-permute-start = (bf16[30,512]{1,0:T(8,128)(2,1)S(1)}, bf16[30,512]{1,0:T(8,128)(2,1)S(1)}, u32[]{:S(2)}, u32[]{:S(2)}) collective-permute-start(bf16[30,512]{1,0:T(8,128)(2,1)S(1)} %slice.252), channel_id=1, source_target_pairs={{0,4},{4,8},{8,12},{12,16},{16,20},{20,24},{24,28},{1,5},{5,9},{9,... | collective-permute-start | bytes 92168 | tf_op jit(solution)/shard_map/ppermute | solution.py:12
  52.9 1.0 fusion.20
  53.9 0.6 collective-permute-done
  54.5 0.2 maximum_convert_fusion
  54.6 5.7 %multiply_reduce_fusion = (f32[512]{0:T(512)S(1)}, f32[512,512]{1,0:T(8,128)}) fusion(f32[542,512]{1,0:T(8,128)S(1)} %maximum_convert_fusion, f32[512]{0:T(512)S(1)} %bitcast.72, f32[512]{0:T(512)S(1)} %bitcast.73, f32[512]{0:T(512)S(1)} %bitcast.75, f32[512]{0:T(512)S(1)} %bitcast.76, f32[512]{0:T(512)S(1)} %bitcast.77, f32[512]{0:T(512)S(1)} %bitcast.78, ...), kind=kLoop, calls=%fused_computation.98 | loop fusion | flops 16514560 | bytes 33619968 | tf_op jit(solution)/shard_map/reduce_sum | solution.py:147
  60.3 6.1 %psum.7 = f32[512]{0:T(512)S(1)} all-reduce(f32[512]{0:T(512)S(1)} %get-tuple-element.390), channel_id=1, replica_groups=mesh['sp'=8,'tp'=4] {'tp'}, use_global_device_ids=true, to_apply=%region_8.9 | all-reduce | flops 512 | bytes 4096 | tf_op jit(solution)/shard_map/psum | solution.py:147
  66.4 23.3 %all-gather.6.cloned.1.call-done = bf16[4096,256]{1,0:T(8,128)(2,1)} async-done(((bf16[512,256]{1,0:T(8,128)(2,1)}), bf16[4096,256]{1,0:T(8,128)(2,1)}) %all-gather.6.cloned.1.call-update) | async-done | bytes 2097168 | tf_op jit(solution)/shard_map/all_gather | solution.py:103
  89.7 4.1 %copy.15 = bf16[4096,256]{0,1:T(8,128)(2,1)} copy(bf16[4096,256]{1,0:T(8,128)(2,1)} %all-gather.6.cloned.1.call-done) | data formatting | bytes 4194304
  93.8 45.7 %all-gather.8.cloned.1.call-done = bf16[4096,256]{1,0:T(8,128)(2,1)} async-done(((bf16[512,256]{1,0:T(8,128)(2,1)}), bf16[4096,256]{1,0:T(8,128)(2,1)}) %all-gather.8.cloned.1.call-update) | async-done | bytes 2097168 | tf_op jit(solution)/shard_map/all_gather | solution.py:104
  139.5 4.1 %copy.16 = bf16[4096,256]{0,1:T(8,128)(2,1)} copy(bf16[4096,256]{1,0:T(8,128)(2,1)} %all-gather.8.cloned.1.call-done) | data formatting | bytes 4194304
  143.7 6.8 %while.18 = (s32[]{:T(128)}, f32[4,512]{1,0:T(4,128)S(1)}, f32[4,512]{1,0:T(4,128)S(1)}, f32[4,512,64]{1,2,0:T(8,128)S(1)}, s32[]{:T(128)}, /*index=5*/bf16[4096...) while((s32[]{:T(128)}, f32[4,512]{1,0:T(4,128)S(1)}, ...), condition=%wide.region_6.7_spmd.clone, body=%wide.region_1.6_spmd.clone.sunk | while | flops 286005248 | bytes 16725373 | solution.py:125
  143.8 6.3 %conditional.3 = ((f32[4,512]{1,0:T(4,128)S(1)}, f32[4,512]{1,0:T(4,128)S(1)}, f32[4,512,64]{1,2,0:T(8,128)S(1)})) conditional(s32[]{:T(128)} %convert_element_type.89, (f32[4,512]{1,0:T(4,128)S(1)}, f32[4,512]{1,0:T(4,128)S(1)}, f32[4,512,64]{1,2,0:T(8,128)S(1)}) %tuple.88, (s32[]{:T(128)}, s32[]{:T(128)}, bf16[4096,256]{0,1:T(8,128)(2,1)}, ...), branch_computations={%region_2.0_spmd, %region_3.5_spmd} | conditional | flops 286005248 | bytes 16723030 | solution.py:122
  143.8 0.2 compare_and_fusion
  144.1 0.7 constant_dynamic-slice_fusion.1
  144.8 1.1 constant_dynamic-slice_fusion
  145.8 1.2 fusion.4
  147.0 1.4 fusion.3
  148.4 1.6 fusion.8
  150.5 0.0 copy-start.8
  150.5 0.1 divide_convert_fusion
  150.6 2.0 fusion.63
  152.7 2.8 %add_convert_fusion = bf16[512,2048]{1,0:T(8,128)(2,1)} fusion(f32[512,2048]{1,0:T(8,128)S(1)} %fusion.63, bf16[512,2048]{1,0:T(8,128)(2,1)S(1)} %copy-done, f32[512,512]{1,0:T(8,128)S(1)} %copy-done.2, f32[512]{0:T(512)S(1)} %copy-done.8, f32[512]{0:T(512)S(1)} %add_rsqrt_fusion), kind=kOutput, calls=%fused_computation.25 | convolution fusion | flops 1077673984 | bytes 9441280 | tf_op jit(solution)/shard_map/dot_general | solution.py:152
  155.5 0.0 reduce-scatter.2.cloned.1.call-update
  155.5 0.6 log_add_fusion
  156.1 73.3 %reduce-scatter.2.cloned.1.call-done = bf16[128,2048]{1,0:T(8,128)(2,1)} async-done(((bf16[512,2048]{1,0:T(8,128)(2,1)}), bf16[128,2048]{1,0:T(8,128)(2,1)}) %reduce-scatter.2.cloned.1.call-update) | async-done | bytes 524304 | tf_op jit(solution)/shard_map/reduce_scatter | solution.py:153
  (36 shorter events, 0.3 us)
Async XLA Ops:
  7.2 145.5 %copy-start = (bf16[512,2048]{1,0:T(8,128)(2,1)S(1)}, bf16[512,2048]{1,0:T(8,128)(2,1)}, u32[]{:S(2)}) copy-start(bf16[512,2048]{1,0:T(8,128)(2,1)} %param.27) | copy-start | bytes 6291460
  7.2 27.7 %all-gather.4.cloned.1.call-start = ((), (), s32[]{:S(2)}) async-start(), calls=%async_computation.1 | async-start | bytes 2621440 | tf_op jit(solution)/shard_map/all_gather | solution.py:33
  7.9 32.5 %copy-start.5 = (bf16[2048,256]{1,0:T(8,128)(2,1)S(1)}, bf16[2048,256]{1,0:T(8,128)(2,1)}, u32[]{:S(2)}) copy-start(bf16[2048,256]{1,0:T(8,128)(2,1)} %param.20) | copy-start | bytes 3145732
  7.9 32.5 %copy-start.7 = (f32[2048]{0:T(1024)S(1)}, f32[2048]{0:T(1024)}, u32[]{:S(2)}) copy-start(f32[2048]{0:T(1024)} %param.17) | copy-start | bytes 24580
  7.9 81.8 %all-gather.6.cloned.1.call-start = ((), (), s32[]{:S(2)}) async-start(), calls=%async_computation.2 | async-start | bytes 2359296 | tf_op jit(solution)/shard_map/all_gather | solution.py:103
  40.3 3.9 %copy-start.3 = (f32[31,512]{1,0:T(8,128)S(1)}, f32[31,512]{1,0:T(8,128)}, u32[]{:S(2)}) copy-start(f32[31,512]{1,0:T(8,128)} %param.23) | copy-start | bytes 190468
  40.3 99.2 %all-gather.8.cloned.1.call-start = ((), (), s32[]{:S(2)}) async-start(), calls=%async_computation.3 | async-start | bytes 2359296 | tf_op jit(solution)/shard_map/all_gather | solution.py:104
  43.5 186.0 %reduce-scatter.2.cloned.1.call-start = ((), (), s32[]{:S(2)}) async-start(), calls=%async_computation.4 | async-start | bytes 2621440 | tf_op jit(solution)/shard_map/reduce_scatter | solution.py:153
  44.3 3.8 %copy-start.1 = (bf16[512,2048]{1,0:T(8,128)(2,1)S(1)}, bf16[512,2048]{1,0:T(8,128)(2,1)}, u32[]{:S(2)}) copy-start(bf16[512,2048]{1,0:T(8,128)(2,1)} %all-gather.4.cloned.1.call-done) | copy-start | bytes 6291460
  44.3 3.8 %copy-start.4 = (bf16[2048,512]{1,0:T(8,128)(2,1)S(1)}, bf16[2048,512]{1,0:T(8,128)(2,1)}, u32[]{:S(2)}) copy-start(bf16[2048,512]{1,0:T(8,128)(2,1)} %param.21) | copy-start | bytes 6291460
  48.1 4.7 %copy-start.6 = (bf16[2048,256]{1,0:T(8,128)(2,1)S(1)}, bf16[2048,256]{1,0:T(8,128)(2,1)}, u32[]{:S(2)}) copy-start(bf16[2048,256]{1,0:T(8,128)(2,1)} %param.18) | copy-start | bytes 3145732
  49.5 5.0 %collective-permute-start = (bf16[30,512]{1,0:T(8,128)(2,1)S(1)}, bf16[30,512]{1,0:T(8,128)(2,1)S(1)}, u32[]{:S(2)}, u32[]{:S(2)}) collective-permute-start(bf16[30,512]{1,0:T(8,128)(2,1)S(1)} %slice.252), channel_id=1, source_target_pairs={{0,4},{4,8},{8,12},{12,16},{16,20},{20,24},{24,28},{1,5},{5,9},{9,... | collective-permute-start | bytes 92168 | tf_op jit(solution)/shard_map/ppermute | solution.py:12
  150.5 2.1 copy-start.2
  150.5 2.1 copy-start.8
Sparse Core Ops, SparseCore 0:
  9.5 25.2 all-gather.3
  40.4 49.2 all-gather.5
  91.9 47.6 all-gather.7
  155.6 73.7 reduce-scatter.1
where the time goes:
time: 237 us; the launch traced here: 236 us
  waiting for transfers between devices  171 us (72%)
  matrix products  20.1 us (8%)
  between operations  14 us (6%)
  local copies, waits for them, and re-layouts  10.9 us (5%)
  other arithmetic  10.3 us (4%)
  blocking collectives  6.08 us (3%)
  starting transfers between devices  3.54 us (1%)
    reduce_scatter x1, waiting for transfers between devices, per_device(): lax.psum_scatter(lax.optimization_barrier(group_part.astype(jnp.bfloat16)...  73.3 us
    all_gather x1, waiting for transfers between devices, per_device(): value_group = lax.all_gather(value_rows, 'sp', axis=0, tiled=True)  45.7 us
    all_gather x1, waiting for transfers between devices, per_device(): wide = lax.all_gather(tokens, 'tp', axis=0, tiled=True).astype(jnp.float32)  26.9 us
    all_gather x1, waiting for transfers between devices, per_device(): key_group = lax.all_gather(key_rows, 'sp', axis=0, tiled=True)  23.3 us
    unnamed x20, local copies, waits for them, and re-layouts  8.28 us
    psum x1, blocking collectives, per_device(): lax.psum(jnp.sum(convolved * convolved, axis=1), 'tp') / all_channels  6.08 us
    reduce_sum x1, other arithmetic, per_device(): jnp.sum(convolved * convolved, axis=1)  5.69 us
  transfers between devices with their start and end apart: 5, of which 5 were waited for; matrix products, arithmetic and copies ran while one was open for 9% of the time, Pallas kernels for 0%

commit v1 on v0

--- a/solution.py
+++ b/solution.py
@@ -101,7 +101,14 @@
         )
     )
     key_group = lax.all_gather(key_rows, "sp", axis=0, tiled=True)
-    value_group = lax.all_gather(value_rows, "sp", axis=0, tiled=True)
+    peers = lax.axis_size("sp")
+    right = [(i_2, (i_2 + 1) % peers) for i_2 in range(peers)]
+    blocks = [value_rows]
+    for far in range(1, peers):
+        blocks = [lax.ppermute(blocks[0], "sp", right), *blocks]
+    result = jnp.concatenate(blocks, axis=0)
+    places = (lax.axis_index("sp") + 1) * blocks[-1].shape[0]
+    value_group = jnp.roll(result, places, axis=0)
     length_in = key_group.shape[0]
     turns = length_in // local_rows
 

time: 237 us -> 230 us (0.970)
  waiting for transfers between devices: 171 us -> 157 us
  local copies, waits for them, and re-layouts: 10.9 us -> 17.5 us
    ppermute x0 -> x7, waiting for transfers between devices: none -> 57.2 us  [per_device(): blocks = [lax.ppermute(blocks[0], 'sp', right), *blocks]]
    all_gather x1 -> x0, waiting for transfers between devices: 45.7 us -> none  [per_device(): value_group = lax.all_gather(value_rows, 'sp', axis=0, tiled=True)]
    all_gather x1, waiting for transfers between devices: 23.3 us -> 0.01 us  [per_device(): key_group = lax.all_gather(key_rows, 'sp', axis=0, tiled=True)]
    unnamed x20 -> x39, local copies, waits for them, and re-layouts: 8.28 us -> 13.3 us
  transfers between devices with their start and end apart: 5 -> 11, of which waited for: 5 -> 9; matrix products, arithmetic and copies ran while one was open for 9% -> 12% of each run, Pallas kernels for 0% -> 0%
where the time goes in v1:
time: 230 us; the launch traced here: 229 us
  waiting for transfers between devices  157 us (68%)
  matrix products  20.4 us (9%)
  local copies, waits for them, and re-layouts  17.5 us (8%)
  between operations  14.1 us (6%)
  other arithmetic  10.2 us (4%)
  blocking collectives  6.22 us (3%)
  starting transfers between devices  2.94 us (1%)
    reduce_scatter x1, waiting for transfers between devices, per_device(): lax.psum_scatter(lax.optimization_barrier(group_part.astype(jnp.bfloat16)...  72.2 us
    ppermute x7, waiting for transfers between devices, per_device(): blocks = [lax.ppermute(blocks[0], 'sp', right), *blocks]  57.2 us
    all_gather x1, waiting for transfers between devices, per_device(): wide = lax.all_gather(tokens, 'tp', axis=0, tiled=True).astype(jnp.float32)  26.9 us
    unnamed x39, local copies, waits for them, and re-layouts  13.3 us
    psum x1, blocking collectives, per_device(): lax.psum(jnp.sum(convolved * convolved, axis=1), 'tp') / all_channels  6.22 us
    reduce_sum x1, other arithmetic, per_device(): jnp.sum(convolved * convolved, axis=1)  5.58 us
  transfers between devices with their start and end apart: 11, of which 9 were waited for; matrix products, arithmetic and copies ran while one was open for 12% of the time, Pallas kernels for 0%

profile of v1, /device:TPU:0, one launch (start us, length us, event | category | flops | bytes accessed | tf_op | source)
XLA Modules:
  0.0 228.7 jit_solution(8539127337218910620)
XLA Ops:
  7.2 0.0 copy-start
  7.2 0.0 all-gather.3.cloned.1.call-start
  7.2 0.7 all-gather.3.cloned.1.call-update
  7.9 0.0 all-gather.5.cloned.1.call-start
  8.0 26.9 %all-gather.3.cloned.1.call-done = bf16[512,2048]{1,0:T(8,128)(2,1)} async-done(((bf16[128,2048]{1,0:T(8,128)(2,1)}), bf16[512,2048]{1,0:T(8,128)(2,1)}) %all-gather.3.cloned.1.call-update) | async-done | bytes 2097168 | tf_op jit(solution)/shard_map/all_gather | solution.py:33
  34.9 2.1 fusion.13
  37.0 2.6 %convolution_convert_fusion = bf16[512,256]{1,0:T(8,128)(2,1)S(1)} fusion(bf16[2048,256]{1,0:T(8,128)(2,1)} %param.20, bf16[512,2048]{1,0:T(8,128)(2,1)} %all-gather.3.cloned.1.call-done, f32[2048]{0:T(1024)} %param.17, f32[512]{0:T(512)S(1)} %add_rsqrt_fusion.1), kind=kOutput, calls=%fused_computation.34 | convolution fusion | flops 541196288 | bytes 3418112 | tf_op jit(solution)/shard_map/dot_general | solution.py:40
  39.6 1.5 collective-permute-start
  41.2 9.6 %collective-permute-done = bf16[512,256]{1,0:T(8,128)(2,1)S(1)} collective-permute-done((bf16[512,256]{1,0:T(8,128)(2,1)S(1)}, bf16[512,256]{1,0:T(8,128)(2,1)S(1)}, u32[]{:S(2)}, u32[]{:S(2)}) %collective-permute-start) | collective-permute-done | bytes 262176 | tf_op jit(solution)/shard_map/ppermute | solution.py:108
  50.8 0.7 constant_dynamic-slice_fusion.4
  51.5 9.6 %collective-permute-done.1 = bf16[512,256]{1,0:T(8,128)(2,1)S(1)} collective-permute-done((bf16[512,256]{1,0:T(8,128)(2,1)S(1)}, bf16[512,256]{1,0:T(8,128)(2,1)S(1)}, u32[]{:S(2)}, u32[]{:S(2)}) %collective-permute-start.1) | collective-permute-done | bytes 262176 | tf_op jit(solution)/shard_map/ppermute | solution.py:108
  61.1 3.3 %convolution_convert_fusion.1 = bf16[512,256]{1,0:T(8,128)(2,1)} fusion(bf16[2048,256]{1,0:T(8,128)(2,1)} %param.19, bf16[512,2048]{1,0:T(8,128)(2,1)} %all-gather.3.cloned.1.call-done, f32[2048]{0:T(1024)S(1)} %copy-done.8, f32[512]{0:T(512)S(1)} %add_rsqrt_fusion.1), kind=kOutput, calls=%fused_computation.35 | convolution fusion | flops 541196288 | bytes 3418112 | tf_op jit(solution)/shard_map/dot_general | solution.py:39
  64.4 0.0 all-gather.5.cloned.1.call-update
  64.4 0.0 reduce-scatter.2.cloned.1.call-start
  64.5 6.0 %collective-permute-done.2 = bf16[512,256]{1,0:T(8,128)(2,1)S(1)} collective-permute-done((bf16[512,256]{1,0:T(8,128)(2,1)S(1)}, bf16[512,256]{1,0:T(8,128)(2,1)S(1)}, u32[]{:S(2)}, u32[]{:S(2)}) %collective-permute-start.2) | collective-permute-done | bytes 262176 | tf_op jit(solution)/shard_map/ppermute | solution.py:108
  70.5 3.8 %fusion.18 = f32[512,512]{1,0:T(8,128)S(1)} fusion(bf16[2048,512]{1,0:T(8,128)(2,1)} %param.22, bf16[512,2048]{1,0:T(8,128)(2,1)} %all-gather.3.cloned.1.call-done, f32[2048]{0:T(1024)S(1)} %copy-done.8, f32[512]{0:T(512)S(1)} %add_rsqrt_fusion.1), kind=kOutput, calls=%fused_computation.30 | convolution fusion | flops 1078722560 | bytes 5253120 | tf_op jit(solution)/shard_map/dot_general | solution.py:42
  74.3 7.1 %collective-permute-done.3 = bf16[512,256]{1,0:T(8,128)(2,1)S(1)} collective-permute-done((bf16[512,256]{1,0:T(8,128)(2,1)S(1)}, bf16[512,256]{1,0:T(8,128)(2,1)S(1)}, u32[]{:S(2)}, u32[]{:S(2)}) %collective-permute-start.3) | collective-permute-done | bytes 262176 | tf_op jit(solution)/shard_map/ppermute | solution.py:108
  81.4 1.3 fusion.19
  82.8 1.3 collective-permute-start.7
  84.1 9.6 %collective-permute-done.4 = bf16[512,256]{1,0:T(8,128)(2,1)S(1)} collective-permute-done((bf16[512,256]{1,0:T(8,128)(2,1)S(1)}, bf16[512,256]{1,0:T(8,128)(2,1)S(1)}, u32[]{:S(2)}, u32[]{:S(2)}) %collective-permute-start.4) | collective-permute-done | bytes 262176 | tf_op jit(solution)/shard_map/ppermute | solution.py:108
  93.6 1.6 fusion.20
  95.3 0.2 maximum_convert_fusion
  95.5 12.5 %collective-permute-done.5 = bf16[512,256]{1,0:T(8,128)(2,1)} collective-permute-done((bf16[512,256]{1,0:T(8,128)(2,1)S(1)}, bf16[512,256]{1,0:T(8,128)(2,1)}, u32[]{:S(2)}, u32[]{:S(2)}) %collective-permute-start.5) | collective-permute-done | bytes 262176 | tf_op jit(solution)/shard_map/ppermute | solution.py:108
  108.0 5.6 %multiply_reduce_fusion = (f32[512]{0:T(512)S(1)}, f32[512,512]{1,0:T(8,128)}) fusion(f32[542,512]{1,0:T(8,128)S(1)} %maximum_convert_fusion, f32[512]{0:T(512)S(1)} %bitcast.72, f32[512]{0:T(512)S(1)} %bitcast.73, f32[512]{0:T(512)S(1)} %bitcast.75, f32[512]{0:T(512)S(1)} %bitcast.76, f32[512]{0:T(512)S(1)} %bitcast.77, f32[512]{0:T(512)S(1)} %bitcast.78, ...), kind=kLoop, calls=%fused_computation.98 | loop fusion | flops 16514560 | bytes 33619968 | tf_op jit(solution)/shard_map/reduce_sum | solution.py:154
  113.6 6.2 %psum.7 = f32[512]{0:T(512)S(1)} all-reduce(f32[512]{0:T(512)S(1)} %get-tuple-element.390), channel_id=1, replica_groups=mesh['sp'=8,'tp'=4] {'tp'}, use_global_device_ids=true, to_apply=%region_8.9 | all-reduce | flops 512 | bytes 4096 | tf_op jit(solution)/shard_map/psum | solution.py:154
  119.8 2.8 %collective-permute-done.6 = bf16[512,256]{1,0:T(8,128)(2,1)} collective-permute-done((bf16[512,256]{1,0:T(8,128)(2,1)}, bf16[512,256]{1,0:T(8,128)(2,1)}, u32[]{:S(2)}, u32[]{:S(2)}) %collective-permute-start.6) | collective-permute-done | bytes 262176 | tf_op jit(solution)/shard_map/ppermute | solution.py:108
  122.6 1.0 constant_dynamic-update-slice_fusion.15
  123.6 1.0 constant_dynamic-update-slice_fusion.14
  124.5 1.0 constant_dynamic-update-slice_fusion.13
  125.6 1.0 constant_dynamic-update-slice_fusion.7
  126.6 1.0 constant_dynamic-update-slice_fusion.6
  127.8 1.5 constant_dynamic-slice_fusion.3
  129.3 4.2 %copy.16 = bf16[4096,256]{0,1:T(8,128)(2,1)} copy(bf16[4096,256]{1,0:T(8,128)(2,1)} %constant_dynamic-slice_fusion.3) | data formatting | bytes 4194304
  133.4 4.1 %copy.15 = bf16[4096,256]{0,1:T(8,128)(2,1)} copy(bf16[4096,256]{1,0:T(8,128)(2,1)} %all-gather.5.cloned.1.call-done) | data formatting | bytes 4194304
  137.6 6.8 %while.18 = (s32[]{:T(128)}, f32[4,512]{1,0:T(4,128)S(1)}, f32[4,512]{1,0:T(4,128)S(1)}, f32[4,512,64]{1,2,0:T(8,128)S(1)}, s32[]{:T(128)}, /*index=5*/bf16[4096...) while((s32[]{:T(128)}, f32[4,512]{1,0:T(4,128)S(1)}, ...), condition=%wide.region_6.7_spmd.clone, body=%wide.region_1.6_spmd.clone.sunk | while | flops 286005248 | bytes 16725373 | solution.py:132
  137.6 6.3 %conditional.3 = ((f32[4,512]{1,0:T(4,128)S(1)}, f32[4,512]{1,0:T(4,128)S(1)}, f32[4,512,64]{1,2,0:T(8,128)S(1)})) conditional(s32[]{:T(128)} %convert_element_type.89, (f32[4,512]{1,0:T(4,128)S(1)}, f32[4,512]{1,0:T(4,128)S(1)}, f32[4,512,64]{1,2,0:T(8,128)S(1)}) %tuple.88, (s32[]{:T(128)}, s32[]{:T(128)}, bf16[4096,256]{0,1:T(8,128)(2,1)}, ...), branch_computations={%region_2.2_spmd, %region_3.5_spmd} | conditional | flops 286005248 | bytes 16723030 | solution.py:129
  137.7 0.2 compare_and_fusion
  137.9 0.7 constant_dynamic-slice_fusion.1
  138.6 1.1 constant_dynamic-slice_fusion
  139.7 1.2 fusion.4
  140.9 1.4 fusion.3
  142.3 1.6 fusion.8
  144.4 0.1 divide_convert_fusion
  144.5 2.0 fusion.63
  146.5 2.8 %add_convert_fusion = bf16[512,2048]{1,0:T(8,128)(2,1)} fusion(f32[512,2048]{1,0:T(8,128)S(1)} %fusion.63, bf16[512,2048]{1,0:T(8,128)(2,1)S(1)} %copy-done, f32[512,512]{1,0:T(8,128)S(1)} %copy-done.2, f32[512]{0:T(512)S(1)} %copy-done.9, f32[512]{0:T(512)S(1)} %add_rsqrt_fusion), kind=kOutput, calls=%fused_computation.25 | convolution fusion | flops 1077673984 | bytes 9441280 | tf_op jit(solution)/shard_map/dot_general | solution.py:159
  149.4 0.0 reduce-scatter.2.cloned.1.call-update
  149.4 0.6 log_add_fusion
  150.0 72.2 %reduce-scatter.2.cloned.1.call-done = bf16[128,2048]{1,0:T(8,128)(2,1)} async-done(((bf16[512,2048]{1,0:T(8,128)(2,1)}), bf16[128,2048]{1,0:T(8,128)(2,1)}) %reduce-scatter.2.cloned.1.call-update) | async-done | bytes 524304 | tf_op jit(solution)/shard_map/reduce_scatter | solution.py:160
  (68 shorter events, 0.6 us)
Async XLA Ops:
  7.2 139.3 %copy-start = (bf16[512,2048]{1,0:T(8,128)(2,1)S(1)}, bf16[512,2048]{1,0:T(8,128)(2,1)}, u32[]{:S(2)}) copy-start(bf16[512,2048]{1,0:T(8,128)(2,1)} %param.27) | copy-start | bytes 6291460
  7.2 34.0 %copy-start.5 = (f32[31,512]{1,0:T(8,128)S(1)}, f32[31,512]{1,0:T(8,128)}, u32[]{:S(2)}) copy-start(f32[31,512]{1,0:T(8,128)} %param.23) | copy-start | bytes 190468
  7.2 27.7 %all-gather.3.cloned.1.call-start = ((), (), s32[]{:S(2)}) async-start(), calls=%async_computation.1 | async-start | bytes 2621440 | tf_op jit(solution)/shard_map/all_gather | solution.py:33
  7.9 53.2 %copy-start.8 = (f32[2048]{0:T(1024)S(1)}, f32[2048]{0:T(1024)}, u32[]{:S(2)}) copy-start(f32[2048]{0:T(1024)} %param.17) | copy-start | bytes 24580
  7.9 125.5 %all-gather.5.cloned.1.call-start = ((), (), s32[]{:S(2)}) async-start(), calls=%async_computation.2 | async-start | bytes 2359296 | tf_op jit(solution)/shard_map/all_gather | solution.py:103
  39.6 11.2 %collective-permute-start = (bf16[512,256]{1,0:T(8,128)(2,1)S(1)}, bf16[512,256]{1,0:T(8,128)(2,1)S(1)}, u32[]{:S(2)}, u32[]{:S(2)}) collective-permute-start(bf16[512,256]{1,0:T(8,128)(2,1)S(1)} %convolution_convert_fusion), channel_id=1, source_target_pairs={{0,4},{4,8},{8,12},{12,16},{16,20},{20,24},{24,28},{28,0},{1,5},{5... | collective-permute-start | bytes 786440 | tf_op jit(solution)/shard_map/ppermute | solution.py:108
  50.8 10.3 %collective-permute-start.1 = (bf16[512,256]{1,0:T(8,128)(2,1)S(1)}, bf16[512,256]{1,0:T(8,128)(2,1)S(1)}, u32[]{:S(2)}, u32[]{:S(2)}) collective-permute-start(bf16[512,256]{1,0:T(8,128)(2,1)S(1)} %collective-permute-done), channel_id=1, source_target_pairs={{0,4},{4,8},{8,12},{12,16},{16,20},{20,24},{24,28},{28,0},{1,5},{5... | collective-permute-start | bytes 786440 | tf_op jit(solution)/shard_map/ppermute | solution.py:108
  61.1 9.4 %collective-permute-start.2 = (bf16[512,256]{1,0:T(8,128)(2,1)S(1)}, bf16[512,256]{1,0:T(8,128)(2,1)S(1)}, u32[]{:S(2)}, u32[]{:S(2)}) collective-permute-start(bf16[512,256]{1,0:T(8,128)(2,1)S(1)} %collective-permute-done.1), channel_id=1, source_target_pairs={{0,4},{4,8},{8,12},{12,16},{16,20},{20,24},{24,28},{28,0},{1,5},{5... | collective-permute-start | bytes 786440 | tf_op jit(solution)/shard_map/ppermute | solution.py:108
  64.4 157.8 %reduce-scatter.2.cloned.1.call-start = ((), (), s32[]{:S(2)}) async-start(), calls=%async_computation.3 | async-start | bytes 2621440 | tf_op jit(solution)/shard_map/reduce_scatter | solution.py:160
  64.5 16.9 %copy-start.1 = (bf16[512,2048]{1,0:T(8,128)(2,1)S(1)}, bf16[512,2048]{1,0:T(8,128)(2,1)}, u32[]{:S(2)}) copy-start(bf16[512,2048]{1,0:T(8,128)(2,1)} %all-gather.3.cloned.1.call-done) | copy-start | bytes 6291460
  64.5 16.9 %copy-start.6 = (bf16[2048,512]{1,0:T(8,128)(2,1)S(1)}, bf16[2048,512]{1,0:T(8,128)(2,1)}, u32[]{:S(2)}) copy-start(bf16[2048,512]{1,0:T(8,128)(2,1)} %param.21) | copy-start | bytes 6291460
  70.5 10.9 %collective-permute-start.3 = (bf16[512,256]{1,0:T(8,128)(2,1)S(1)}, bf16[512,256]{1,0:T(8,128)(2,1)S(1)}, u32[]{:S(2)}, u32[]{:S(2)}) collective-permute-start(bf16[512,256]{1,0:T(8,128)(2,1)S(1)} %collective-permute-done.2), channel_id=1, source_target_pairs={{0,4},{4,8},{8,12},{12,16},{16,20},{20,24},{24,28},{28,0},{1,5},{5... | collective-permute-start | bytes 786440 | tf_op jit(solution)/shard_map/ppermute | solution.py:108
  74.3 19.4 %copy-start.7 = (bf16[2048,256]{1,0:T(8,128)(2,1)S(1)}, bf16[2048,256]{1,0:T(8,128)(2,1)}, u32[]{:S(2)}) copy-start(bf16[2048,256]{1,0:T(8,128)(2,1)} %param.18) | copy-start | bytes 3145732
  81.4 12.2 %collective-permute-start.4 = (bf16[512,256]{1,0:T(8,128)(2,1)S(1)}, bf16[512,256]{1,0:T(8,128)(2,1)S(1)}, u32[]{:S(2)}, u32[]{:S(2)}) collective-permute-start(bf16[512,256]{1,0:T(8,128)(2,1)S(1)} %collective-permute-done.3), channel_id=1, source_target_pairs={{0,4},{4,8},{8,12},{12,16},{16,20},{20,24},{24,28},{28,0},{1,5},{5... | collective-permute-start | bytes 786440 | tf_op jit(solution)/shard_map/ppermute | solution.py:108
  82.8 12.5 %collective-permute-start.7 = (bf16[30,512]{1,0:T(8,128)(2,1)S(1)}, bf16[30,512]{1,0:T(8,128)(2,1)S(1)}, u32[]{:S(2)}, u32[]{:S(2)}) collective-permute-start(bf16[30,512]{1,0:T(8,128)(2,1)S(1)} %slice.252), channel_id=1, source_target_pairs={{0,4},{4,8},{8,12},{12,16},{16,20},{20,24},{24,28},{1,5},{5,9},{9,... | collective-permute-start | bytes 92168 | tf_op jit(solution)/shard_map/ppermute | solution.py:12
  93.6 19.9 %copy-start.3 = (bf16[512,256]{1,0:T(8,128)(2,1)}, bf16[512,256]{1,0:T(8,128)(2,1)S(1)}, u32[]{:S(2)}) copy-start(bf16[512,256]{1,0:T(8,128)(2,1)S(1)} %collective-permute-done.4) | copy-start | bytes 786436
  93.6 14.3 %collective-permute-start.5 = (bf16[512,256]{1,0:T(8,128)(2,1)S(1)}, bf16[512,256]{1,0:T(8,128)(2,1)}, u32[]{:S(2)}, u32[]{:S(2)}) collective-permute-start(bf16[512,256]{1,0:T(8,128)(2,1)S(1)} %collective-permute-done.4), channel_id=1, source_target_pairs={{0,4},{4,8},{8,12},{12,16},{16,20},{20,24},{24,28},{28,0},{1,5},{5... | collective-permute-start | bytes 786440 | tf_op jit(solution)/shard_map/ppermute | solution.py:108
  108.0 14.6 %collective-permute-start.6 = (bf16[512,256]{1,0:T(8,128)(2,1)}, bf16[512,256]{1,0:T(8,128)(2,1)}, u32[]{:S(2)}, u32[]{:S(2)}) collective-permute-start(bf16[512,256]{1,0:T(8,128)(2,1)} %collective-permute-done.5), channel_id=1, source_target_pairs={{0,4},{4,8},{8,12},{12,16},{16,20},{20,24},{24,28},{28,0},{1,5},{5... | collective-permute-start | bytes 786440 | tf_op jit(solution)/shard_map/ppermute | solution.py:108
  119.8 7.8 %copy-start.4 = (bf16[512,256]{1,0:T(8,128)(2,1)S(1)}, bf16[512,256]{1,0:T(8,128)(2,1)}, u32[]{:S(2)}) copy-start(bf16[512,256]{1,0:T(8,128)(2,1)} %copy-done.3) | copy-start | bytes 786436
  129.3 8.3 %copy-start.10 = (bf16[512,256]{0,1:T(8,128)(2,1)S(1)}, bf16[512,256]{0,1:T(8,128)(2,1)}, u32[]{:S(2)}) copy-start(bf16[512,256]{0,1:T(8,128)(2,1)} %fusion.20) | copy-start | bytes 786436
  144.4 2.1 copy-start.2
  144.4 2.1 copy-start.9
Sparse Core Ops, SparseCore 0:
  9.6 25.2 all-gather.2
  64.5 58.4 all-gather.4
  149.5 72.6 reduce-scatter.1
